TPU v7x, 256 devices: a whole 4x4x8 slice. The times are simulated.
256 devices in a mesh: sp: 64 (over z, y, core), tp: 4 (over x).
Axes of the slice: x: 4, y: 4, z: 8, core: 2. Of those that a mesh axis runs over, the one named last changes fastest.
Arguments:
- resid: bfloat16 [24576, 2048], P(('sp', 'tp')), may hold values from -6 to 6
- conv_b: bfloat16 [24576, 1024], P('sp', 'tp'), may hold values from -6 to 6
- conv_c: bfloat16 [24576, 1024], P('sp', 'tp'), may hold values from -6 to 6
- conv_x: bfloat16 [24576, 1024], P('sp', 'tp'), may hold values from -6 to 6
- conv_taps: bfloat16 [3, 1024], P(None, 'tp'), may hold values from -3.5 to 3.5
- out_weight: bfloat16 [1024, 2048], P('tp'), may hold values from -0.1875 to 0.1875
- norm_gain: float32 [2048], replicated, may hold values from 0.1 to 1.9
- routes: int32 [24576, 2], P('sp'), may hold values from 0 to 63, all different within a row; in each aligned block of 96 rows (0 to 95, 96 to 191, ...) at most 4 rows name the same one
- route_weight: float32 [24576, 2], P('sp'), may hold values from 0.2 to 1
- expert_gate: bfloat16 [64, 2048, 1024], P('sp', None, 'tp'), may hold values from -0.125 to 0.125
- expert_up: bfloat16 [64, 2048, 1024], P('sp', None, 'tp'), may hold values from -0.125 to 0.125
- expert_down: bfloat16 [64, 1024, 2048], P('sp', 'tp'), may hold values from -0.1875 to 0.1875
- shared_gate: bfloat16 [2048, 1024], P(None, 'tp'), may hold values from -0.125 to 0.125
- shared_up: bfloat16 [2048, 1024], P(None, 'tp'), may hold values from -0.125 to 0.125
- shared_down: bfloat16 [1024, 2048], P('tp'), may hold values from -0.1875 to 0.1875
Outputs:
- layer_out: bfloat16 [24576, 2048], P(('sp', 'tp'))
Inputs may be any that keep to these rules, and one draw needn't show every extreme that they name: `routes`: in each aligned block of 96 tokens no expert is named more than 4 times; in some blocks some expert is named exactly 4 times; each row names 2 different experts.
All inputs are finite; a program needn't handle non-finite values.
Results may differ from a plain program's by a relative error of at most 0.015.
Values may be sent and summed in bfloat16 or wider, within the bound.
A program may use at most 128 MiB of HBM per device.

v0:
```python
import jax
import jax.numpy as jnp
from jax import lax
from jax.sharding import PartitionSpec as P


def shifted(block, axis, distance):
    devices = range(lax.axis_size(axis))
    route = [(i - distance, i) for i in devices if i - distance in devices]
    return lax.ppermute(block, axis, route)


def round_trip(values):
    return lax.optimization_barrier(values.astype(jnp.bfloat16)).astype(jnp.float32)


def rank_slots(route_rows, expert_count, tp_parts):
    flat_routes = route_rows.reshape(tp_parts, -1)
    onehot = (
        flat_routes[:, :, None] == jnp.arange(expert_count, dtype=jnp.int32)[None, None, :]
    ).astype(jnp.int32)
    slot_ranks = jnp.sum((jnp.cumsum(onehot, axis=1) - 1) * onehot, axis=2)
    return (flat_routes, slot_ranks)


def local(
    resid,
    conv_b,
    conv_c,
    conv_x,
    conv_taps,
    out_weight,
    norm_gain,
    routes,
    route_weight,
    expert_gate,
    expert_up,
    expert_down,
    shared_gate,
    shared_up,
    shared_down,
):
    tok_dev = conv_b.shape[0]
    tp_parts = lax.axis_size("tp")
    groups = lax.axis_size("sp")
    quarter = tok_dev // tp_parts
    tap_count = conv_taps.shape[0]
    exp_dev = expert_gate.shape[0]
    expert_count = exp_dev * groups
    model_width = resid.shape[1]
    top_count = routes.shape[1]
    capacity = max(2, 3 * quarter * top_count // (2 * expert_count))
    my_part = lax.axis_index("tp")
    product = conv_c.astype(jnp.float32) * conv_x.astype(jnp.float32)
    rim_rows = shifted(product[tok_dev - (tap_count - 1) :], "sp", 1)
    padded = jnp.concatenate([rim_rows, product], 0)
    conv_sum = padded[0:tok_dev] * conv_taps[0].astype(jnp.float32)
    for tap_index in range(1, tap_count):
        conv_sum = conv_sum + padded[tap_index : tap_index + tok_dev] * conv_taps[tap_index].astype(
            jnp.float32
        )
    mixed_rows = (conv_b.astype(jnp.float32) * conv_sum).astype(jnp.bfloat16)
    projected = lax.psum_scatter(
        round_trip(jnp.dot(mixed_rows, out_weight, preferred_element_type=jnp.float32)).astype(
            jnp.bfloat16
        ),
        "tp",
        scatter_dimension=0,
        tiled=True,
    ).astype(jnp.float32)
    middle = (resid.astype(jnp.float32) + projected).astype(jnp.bfloat16)
    middle_float = middle.astype(jnp.float32)
    inv_scale = lax.rsqrt(jnp.mean(middle_float * middle_float, axis=-1, keepdims=True) + 1e-06)
    normed = (middle_float * inv_scale * norm_gain).astype(jnp.bfloat16)
    flat_routes, slot_ranks = rank_slots(routes, expert_count, tp_parts)
    own_routes = lax.dynamic_index_in_dim(flat_routes, my_part, 0, keepdims=False)
    own_ranks = lax.dynamic_index_in_dim(slot_ranks, my_part, 0, keepdims=False)
    slot_ids = own_routes * capacity + own_ranks
    token_ids = jnp.repeat(jnp.arange(quarter, dtype=jnp.int32), top_count)
    slot_token = (
        jnp.full((expert_count * capacity,), quarter, jnp.int32).at[slot_ids].set(token_ids)
    )
    padded_rows = jnp.concatenate([normed, jnp.zeros((1, model_width), jnp.bfloat16)], 0)
    outgoing = padded_rows[slot_token].reshape(groups, exp_dev * capacity, model_width)
    arrived = lax.all_to_all(outgoing, "sp", split_axis=0, concat_axis=0, tiled=True)
    arrived = arrived.reshape(groups, exp_dev, capacity, model_width)
    arrived, group_normed = (
        lax.all_gather(arrived, "tp", axis=2, tiled=True),
        lax.all_gather(normed, "tp", axis=0, tiled=True),
    )
    gate_val = jnp.einsum(
        "gerd,edf->gerf", arrived, expert_gate, preferred_element_type=jnp.float32
    )
    up_val = jnp.einsum("gerd,edf->gerf", arrived, expert_up, preferred_element_type=jnp.float32)
    hidden = (jax.nn.silu(gate_val) * up_val).astype(jnp.bfloat16)
    partial_rows = round_trip(
        jnp.einsum("gerf,efd->gerd", hidden, expert_down, preferred_element_type=jnp.float32)
    )
    shared_gate_val = jnp.dot(group_normed, shared_gate, preferred_element_type=jnp.float32)
    shared_up_val = jnp.dot(group_normed, shared_up, preferred_element_type=jnp.float32)
    shared_hidden = (jax.nn.silu(shared_gate_val) * shared_up_val).astype(jnp.bfloat16)
    shared_part = round_trip(
        jnp.dot(shared_hidden, shared_down, preferred_element_type=jnp.float32)
    )
    summed, shared = (
        lax.psum_scatter(
            partial_rows.astype(jnp.bfloat16), "tp", scatter_dimension=2, tiled=True
        ).astype(jnp.float32),
        lax.psum_scatter(
            shared_part.astype(jnp.bfloat16), "tp", scatter_dimension=0, tiled=True
        ).astype(jnp.float32),
    )
    returned = lax.all_to_all(
        summed.astype(jnp.bfloat16), "sp", split_axis=0, concat_axis=0, tiled=True
    )
    returned = returned.reshape(expert_count * capacity, model_width)
    picked = returned[own_routes * capacity + own_ranks].reshape(quarter, top_count, model_width)
    own_weights = lax.dynamic_slice_in_dim(route_weight, my_part * quarter, quarter, 0)
    routed = jnp.sum(picked.astype(jnp.float32) * own_weights[:, :, None], axis=1)
    return (middle.astype(jnp.float32) + shared + routed).astype(jnp.bfloat16)


def solution(mesh):
    return jax.shard_map(
        local,
        mesh=mesh,
        in_specs=(
            P(("sp", "tp"), None),
            P("sp", "tp"),
            P("sp", "tp"),
            P("sp", "tp"),
            P(None, "tp"),
            P("tp", None),
            P(),
            P("sp", None),
            P("sp", None),
            P("sp", None, "tp"),
            P("sp", None, "tp"),
            P("sp", "tp", None),
            P(None, "tp"),
            P(None, "tp"),
            P("tp", None),
        ),
        out_specs=P(("sp", "tp"), None),
        check_vma=False,
    )
```

profile of v0, /device:TPU:1, one launch (start us, length us, event | category | flops | bytes accessed | tf_op | source)
XLA Modules:
  0.0 281.4 jit_solution(15139405090504358709)
XLA Ops:
  6.5 1.1 convert_multiply_fusion.2
  7.7 4.6 %collective-permute-start = (f32[2,256]{1,0:T(2,128)S(1)}, f32[2,256]{1,0:T(2,128)S(1)}, u32[]{:S(2)}, u32[]{:S(2)}) collective-permute-start(f32[2,256]{1,0:T(2,128)S(1)} %slice.40), channel_id=1, source_target_pairs={{0,4},{4,8},{8,12},{12,16},{16,20},{20,24},{24,28},{28,32},{32,36}... | collective-permute-start | bytes 6152 | tf_op jit(solution)/shard_map/ppermute | solution.py:10
  12.3 0.8 slice_convert_fusion.2
  13.1 3.2 %convolution_convert_fusion.1 = bf16[384,2048]{1,0:T(8,128)(2,1)} fusion(bf16[256,2048]{1,0:T(8,128)(2,1)} %param.20, f32[2,256]{1,0:T(2,128)S(1)} %collective-permute-done, f32[384,256]{1,0:T(8,128)S(1)} %convert_multiply_fusion.2, bf16[384,256]{1,0:T(8,128)(2,1)} %param.16, f32[256]{0:T(256)S(1)} %bitcast.68, f32[256]{0:T(256)S(1)} %bitcast.69, ...), kind=kOutput, calls=%fused_computation.5 | convolution fusion | flops 404422656 | bytes 3216384 | tf_op jit(solution)/shard_map/dot_general | solution.py:64
  16.3 0.0 reduce-scatter.4.cloned.1.call-update
  16.3 0.0 all-gather.6.cloned.1.call-start
  16.3 0.6 copy-done.6
  16.9 0.1 copy.34
  17.1 0.2 reshape.92
  17.3 2.4 reduce-window.6
  19.7 0.1 slice.43
  19.9 0.1 copy.36
  20.0 0.1 reshape.129
  20.2 0.1 bitcast_bitcast_fusion
  20.3 0.1 fusion.26
  20.4 1.2 scatter_custom_fusion
  21.6 26.1 %reduce-scatter.4.cloned.1.call-done = bf16[96,2048]{1,0:T(8,128)(2,1)} async-done(((bf16[384,2048]{1,0:T(8,128)(2,1)}), bf16[96,2048]{1,0:T(8,128)(2,1)}) %reduce-scatter.4.cloned.1.call-update) | async-done | bytes 393232 | tf_op jit(solution)/shard_map/reduce_scatter | solution.py:63
  47.8 1.2 fusion.7
  49.0 1.2 fusion.9
  50.2 0.7 copy-done.3
  50.9 1.4 gather_fusion
  52.3 0.4 reshape.96
  52.8 39.5 %all_to_all.10 = bf16[64,4,2048]{2,1,0:T(4,128)(2,1)S(1)} all-to-all(bf16[64,4,2048]{2,1,0:T(4,128)(2,1)S(1)} %reshape.96), channel_id=1, replica_groups=mesh['sp'=64,'tp'=4] {'sp'}, dimensions={0} | all-to-all | bytes 2097152 | tf_op jit(solution)/shard_map/all_to_all | solution.py:85
  92.2 1.6 copy.39
  93.8 0.0 all-gather.6.cloned.1.call-update
  93.9 0.0 all-gather.4.cloned.1.call-start
  93.9 0.7 all-gather.4.cloned.1.call-update
  94.6 0.0 reduce-scatter.8.cloned.1.call-start
  94.7 45.3 %all-gather.6.cloned.1.call-done = bf16[64,16,2048]{2,0,1:T(8,128)(2,1)} async-done(((bf16[64,4,2048]{2,0,1:T(8,128)(2,1)}), bf16[64,16,2048]{2,0,1:T(8,128)(2,1)}) %all-gather.6.cloned.1.call-update) | async-done | bytes 4194320 | tf_op jit(solution)/shard_map/all_gather | solution.py:88
  140.0 3.6 %convolution_bitcast_fusion.1 = f32[64,1,16,256]{3,0,2,1:T(8,128)S(1)} fusion(bf16[64,16,2048]{2,0,1:T(8,128)(2,1)} %all-gather.6.cloned.1.call-done, bf16[1,2048,256]{2,1,0:T(8,128)(2,1)S(1)} %copy-done.9), kind=kOutput, calls=%fused_computation.9 | convolution fusion | flops 1073741824 | bytes 6291456 | tf_op jit(solution)/shard_map/gerd,edf->gerf/dot_general | solution.py:91
  143.6 1.3 fusion.2
  144.9 1.4 convert_bitcast_fusion
  146.3 4.2 %copy.41 = bf16[64,1,16,2048]{3,0,1,2:T(8,128)(2,1)} copy(bf16[64,1,16,2048]{3,2,0,1:T(8,128)(2,1)S(1)} %convert_bitcast_fusion) | data formatting | bytes 8388608 | tf_op jit(solution)/shard_map/optimization_barrier | solution.py:14
  150.6 0.2 reduce-scatter.6.cloned.1.call-start
  150.8 20.4 %all-gather.4.cloned.1.call-done = bf16[384,2048]{1,0:T(8,128)(2,1)} async-done(((bf16[96,2048]{1,0:T(8,128)(2,1)}), bf16[384,2048]{1,0:T(8,128)(2,1)}) %all-gather.4.cloned.1.call-update) | async-done | bytes 1572880 | tf_op jit(solution)/shard_map/all_gather | solution.py:89
  171.2 2.4 fusion.38
  173.6 4.5 %convolution_convert_fusion = bf16[384,2048]{1,0:T(8,128)(2,1)} fusion(bf16[256,2048]{1,0:T(8,128)(2,1)} %param.29, bf16[384,2048]{1,0:T(8,128)(2,1)S(1)} %copy-done.8, bf16[2048,256]{1,0:T(8,128)(2,1)} %param.28, f32[384,256]{1,0:T(8,128)S(1)} %fusion.38), kind=kOutput, calls=%fused_computation.4 | convolution fusion | flops 806682624 | bytes 5636096 | tf_op jit(solution)/shard_map/dot_general | solution.py:103
  178.2 44.9 %reduce-scatter.8.cloned.1.call-done = bf16[64,1,4,2048]{3,0,1,2:T(8,128)(2,1)} async-done(((bf16[64,1,16,2048]{3,0,1,2:T(8,128)(2,1)}), bf16[64,1,4,2048]{3,0,1,2:T(8,128)(2,1)}) %reduce-scatter.8.cloned.1.call-update) | async-done | bytes 1048592 | tf_op jit(solution)/shard_map/reduce_scatter | solution.py:106
  223.1 3.0 %copy.42 = bf16[64,1,4,2048]{3,2,1,0:T(4,128)(2,1)} copy(bf16[64,1,4,2048]{3,0,1,2:T(8,128)(2,1)} %reduce-scatter.8.cloned.1.call-done) | data formatting | bytes 2097152 | tf_op jit(solution)/shard_map/reduce_scatter | solution.py:106
  226.1 10.8 %all-to-all-start.1 = ((bf16[64,1,4,2048]{3,2,1,0:T(4,128)(2,1)}), bf16[64,1,4,2048]{3,2,1,0:T(4,128)(2,1)S(1)}, u32[]{:S(2)}, u32[]{:S(2)}) async-start(bf16[64,1,4,2048]{3,2,1,0:T(4,128)(2,1)} %copy.42), calls=%async_computation.4 | async-start | bytes 2097152 | tf_op jit(solution)/shard_map/all_to_all | solution.py:113
  236.9 0.8 constant_dynamic-slice_fusion
  237.7 0.7 copy.43
  238.4 26.7 %all-to-all-done.1 = bf16[64,1,4,2048]{3,2,1,0:T(4,128)(2,1)S(1)} async-done(((bf16[64,1,4,2048]{3,2,1,0:T(4,128)(2,1)}), bf16[64,1,4,2048]{3,2,1,0:T(4,128)(2,1)S(1)}, u32[]{:S(2)}, u32[]{:S(2)}) %all-to-all-start.1) | async-done | bytes 1048608 | tf_op jit(solution)/shard_map/all_to_all | solution.py:113
  265.1 0.3 reshape.103
  265.3 2.0 gather_fusion.1
  267.4 2.2 reshape.108
  269.6 3.2 %multiply_reduce_fusion = f32[96,2048]{1,0:T(8,128)} fusion(f32[96,2,2048]{2,1,0:T(2,128)S(1)} %reshape.108, f32[96,2]{1,0:T(8,128)S(1)} %copy-done.4), kind=kLoop, calls=%fused_computation.6 | loop fusion | flops 589824 | bytes 2360064 | tf_op jit(solution)/shard_map/reduce_sum | solution.py:119
  272.7 2.2 fusion.11
  (38 shorter events, 0.2 us)
Async XLA Ops:
  6.5 138.4 %copy-start = (bf16[1,256,2048]{2,1,0:T(8,128)(2,1)S(1)}, bf16[1,256,2048]{2,1,0:T(8,128)(2,1)}, u32[]{:S(2)}) copy-start(bf16[1,256,2048]{2,1,0:T(8,128)(2,1)} %param.26) | copy-start | bytes 3145732
  6.5 41.2 %reduce-scatter.4.cloned.1.call-start = ((), (), s32[]{:S(2)}) async-start(), calls=%async_computation.5 | async-start | bytes 1966080 | tf_op jit(solution)/shard_map/reduce_scatter | solution.py:63
  7.7 5.4 %collective-permute-start = (f32[2,256]{1,0:T(2,128)S(1)}, f32[2,256]{1,0:T(2,128)S(1)}, u32[]{:S(2)}, u32[]{:S(2)}) collective-permute-start(f32[2,256]{1,0:T(2,128)S(1)} %slice.40), channel_id=1, source_target_pairs={{0,4},{4,8},{8,12},{12,16},{16,20},{20,24},{24,28},{28,32},{32,36}... | collective-permute-start | bytes 6152 | tf_op jit(solution)/shard_map/ppermute | solution.py:10
  16.3 0.7 copy-start.6
  16.3 31.5 %copy-start.1 = (bf16[96,2048]{1,0:T(8,128)(2,1)S(1)}, bf16[96,2048]{1,0:T(8,128)(2,1)}, u32[]{:S(2)}) copy-start(bf16[96,2048]{1,0:T(8,128)(2,1)} %param.15) | copy-start | bytes 1179652
  16.3 123.7 %all-gather.6.cloned.1.call-start = ((), (), s32[]{:S(2)}) async-start(), calls=%async_computation.9 | async-start | bytes 5242880 | tf_op jit(solution)/shard_map/all_gather | solution.py:88
  17.3 31.7 %copy-start.5 = (f32[2048]{0:T(1024)S(1)}, f32[2048]{0:T(1024)}, u32[]{:S(2)}) copy-start(f32[2048]{0:T(1024)} %param.21) | copy-start | bytes 24580
  50.2 0.7 copy-start.3
  92.2 47.8 %copy-start.9 = (bf16[1,2048,256]{2,1,0:T(8,128)(2,1)S(1)}, bf16[1,2048,256]{2,1,0:T(8,128)(2,1)}, u32[]{:S(2)}) copy-start(bf16[1,2048,256]{2,1,0:T(8,128)(2,1)} %param.24) | copy-start | bytes 3145732
  93.9 77.3 %all-gather.4.cloned.1.call-start = ((), (), s32[]{:S(2)}) async-start(), calls=%async_computation.6 | async-start | bytes 1966080 | tf_op jit(solution)/shard_map/all_gather | solution.py:89
  94.6 49.0 %copy-start.10 = (bf16[1,2048,256]{2,1,0:T(8,128)(2,1)S(1)}, bf16[1,2048,256]{2,1,0:T(8,128)(2,1)}, u32[]{:S(2)}) copy-start(bf16[1,2048,256]{2,1,0:T(8,128)(2,1)} %param.25) | copy-start | bytes 3145732
  94.6 128.5 %reduce-scatter.8.cloned.1.call-start = ((), (), s32[]{:S(2)}) async-start(), calls=%async_computation.8 | async-start | bytes 5242880 | tf_op jit(solution)/shard_map/reduce_scatter | solution.py:106
  140.0 3.6 %copy-start.7 = (bf16[64,16,2048]{2,0,1:T(8,128)(2,1)S(1)}, bf16[64,16,2048]{2,0,1:T(8,128)(2,1)}, u32[]{:S(2)}) copy-start(bf16[64,16,2048]{2,0,1:T(8,128)(2,1)} %all-gather.6.cloned.1.call-done) | copy-start | bytes 12582916
  150.6 122.2 %reduce-scatter.6.cloned.1.call-start = ((), (), s32[]{:S(2)}) async-start(), calls=%async_computation.7 | async-start | bytes 1966080 | tf_op jit(solution)/shard_map/reduce_scatter | solution.py:109
  171.2 2.4 copy-start.8
  226.1 38.9 %all-to-all-start.1 = ((bf16[64,1,4,2048]{3,2,1,0:T(4,128)(2,1)}), bf16[64,1,4,2048]{3,2,1,0:T(4,128)(2,1)S(1)}, u32[]{:S(2)}, u32[]{:S(2)}) async-start(bf16[64,1,4,2048]{3,2,1,0:T(4,128)(2,1)} %copy.42), calls=%async_computation.4 | async-start | bytes 2097152 | tf_op jit(solution)/shard_map/all_to_all | solution.py:113
  267.4 2.2 copy-start.4
  269.5 3.2 %copy-start.2 = (bf16[96,2048]{1,0:T(8,128)(2,1)S(1)}, bf16[96,2048]{1,0:T(8,128)(2,1)}, u32[]{:S(2)}) copy-start(bf16[96,2048]{1,0:T(8,128)(2,1)} %reduce-scatter.4.cloned.1.call-done) | copy-start | bytes 1179652
Sparse Core Ops, SparseCore 0:
  16.4 31.3 reduce-scatter.3
  94.0 45.9 all-gather.5
  141.8 29.3 all-gather.3
  173.6 49.4 reduce-scatter.7
  225.5 27.2 reduce-scatter.5
where the time goes:
time: 282 us; the launch traced here: 281 us
  waiting for transfers between devices  164 us (58%)
  blocking collectives  39.5 us (14%)
  local copies, waits for them, and re-layouts  19.9 us (7%)
  matrix products  16.3 us (6%)
  starting transfers between devices  15.7 us (6%)
  between operations  13.4 us (5%)
  other arithmetic  12.4 us (4%)
    all_gather x1, waiting for transfers between devices, local(): lax.all_gather(arrived, 'tp', axis=2, tiled=True)  45.3 us
    reduce_scatter x1, waiting for transfers between devices, local(): lax.psum_scatter(partial_rows.astype(jnp.bfloat16), 'tp', scatter_dimensi...  44.9 us
    all_to_all x1, blocking collectives, local(): lax.all_to_all(outgoing, 'sp', split_axis=0, concat_axis=0, tiled=True)  39.5 us
    all_to_all x1, waiting for transfers between devices, local(): lax.all_to_all(summed.astype(jnp.bfloat16), 'sp', split_axis=0, concat_ax...  26.7 us
    reduce_scatter x1, waiting for transfers between devices, local(): lax.psum_scatter(round_trip(jnp.dot(mixed_rows, out_weight, preferred_ele...  26.1 us
    all_gather x1, waiting for transfers between devices, local(): lax.all_gather(normed, 'tp', axis=0, tiled=True)  20.4 us
    all_to_all x1, starting transfers between devices, local(): lax.all_to_all(summed.astype(jnp.bfloat16), 'sp', split_axis=0, concat_ax...  10.8 us
  transfers between devices with their start and end apart: 7, of which 5 were waited for; matrix products, arithmetic and copies ran while one was open for 12% of the time, Pallas kernels for 0%

commit v1 on v0

--- a/solution.py
+++ b/solution.py
@@ -2,6 +2,11 @@
 import jax.numpy as jnp
 from jax import lax
 from jax.sharding import PartitionSpec as P
+
+
+def swapped_in(x, mesh_axis, dim):
+    sent = jnp.stack([x] * lax.axis_size(mesh_axis))
+    return jnp.concatenate(lax.all_to_all(sent, mesh_axis, 0, 0), axis=dim)
 
 
 def shifted(block, axis, distance):
@@ -86,7 +91,7 @@
     arrived = arrived.reshape(groups, exp_dev, capacity, model_width)
     arrived, group_normed = (
         lax.all_gather(arrived, "tp", axis=2, tiled=True),
-        lax.all_gather(normed, "tp", axis=0, tiled=True),
+        swapped_in(normed, "tp", 0),
     )
     gate_val = jnp.einsum(
         "gerd,edf->gerf", arrived, expert_gate, preferred_element_type=jnp.float32

time: 282 us -> 269 us (0.954)
  waiting for transfers between devices: 164 us -> 122 us
  blocking collectives: 39.5 us -> 70.5 us
    all_to_all x0 -> x1, blocking collectives: none -> 31 us  [swapped_in(): return jnp.concatenate(lax.all_to_all(sent, mesh_axis, 0, 0), axis=dim)]
    reduce_scatter x1, waiting for transfers between devices: 44.9 us -> 23 us  [local(): lax.psum_scatter(partial_rows.astype(jnp.bfloat16), 'tp', scatter_dimensi...]
    all_gather x1 -> x0, waiting for transfers between devices: 20.4 us -> none  [local(): lax.all_gather(normed, 'tp', axis=0, tiled=True)]
  transfers between devices with their start and end apart: 7 -> 6, of which waited for: 5 -> 4; matrix products, arithmetic and copies ran while one was open for 12% -> 8% of each run, Pallas kernels for 0% -> 0%
where the time goes in v1:
time: 269 us
  waiting for transfers between devices  122 us (45%)
  blocking collectives  70.5 us (26%)
  local copies, waits for them, and re-layouts  20.9 us (8%)
  starting transfers between devices  15.1 us (6%)
  matrix products  14.5 us (5%)
  between operations  13.4 us (5%)
  other arithmetic  12.4 us (5%)
    all_gather x1, waiting for transfers between devices, local(): lax.all_gather(arrived, 'tp', axis=2, tiled=True)  46.1 us
    all_to_all x1, blocking collectives, local(): lax.all_to_all(outgoing, 'sp', split_axis=0, concat_axis=0, tiled=True)  39.5 us
    all_to_all x1, blocking collectives, swapped_in(): return jnp.concatenate(lax.all_to_all(sent, mesh_axis, 0, 0), axis=dim)  31 us
    all_to_all x1, waiting for transfers between devices, local(): lax.all_to_all(summed.astype(jnp.bfloat16), 'sp', split_axis=0, concat_ax...  26.7 us
    reduce_scatter x1, waiting for transfers between devices, local(): lax.psum_scatter(round_trip(jnp.dot(mixed_rows, out_weight, preferred_ele...  26.1 us
    reduce_scatter x1, waiting for transfers between devices, local(): lax.psum_scatter(partial_rows.astype(jnp.bfloat16), 'tp', scatter_dimensi...  23 us
    all_to_all x1, starting transfers between devices, local(): lax.all_to_all(summed.astype(jnp.bfloat16), 'sp', split_axis=0, concat_ax...  10.4 us
  transfers between devices with their start and end apart: 6, of which 4 were waited for; matrix products, arithmetic and copies ran while one was open for 8% of the time, Pallas kernels for 0%

profile of v1, /device:TPU:1, one launch (start us, length us, event | category | flops | bytes accessed | tf_op | source)
XLA Modules:
  0.0 268.8 jit_solution(6708056348959006757)
XLA Ops:
  6.5 1.1 convert_multiply_fusion.2
  7.7 4.6 %collective-permute-start = (f32[2,256]{1,0:T(2,128)S(1)}, f32[2,256]{1,0:T(2,128)S(1)}, u32[]{:S(2)}, u32[]{:S(2)}) collective-permute-start(f32[2,256]{1,0:T(2,128)S(1)} %slice.40), channel_id=1, source_target_pairs={{0,4},{4,8},{8,12},{12,16},{16,20},{20,24},{24,28},{28,32},{32,36}... | collective-permute-start | bytes 6152 | tf_op jit(solution)/shard_map/ppermute | solution.py:15
  12.3 0.8 slice_convert_fusion.2
  13.1 3.2 %convolution_convert_fusion.1 = bf16[384,2048]{1,0:T(8,128)(2,1)} fusion(bf16[256,2048]{1,0:T(8,128)(2,1)} %param.20, f32[2,256]{1,0:T(2,128)S(1)} %collective-permute-done, f32[384,256]{1,0:T(8,128)S(1)} %convert_multiply_fusion.2, bf16[384,256]{1,0:T(8,128)(2,1)} %param.16, f32[256]{0:T(256)S(1)} %bitcast.71, f32[256]{0:T(256)S(1)} %bitcast.72, ...), kind=kOutput, calls=%fused_computation.5 | convolution fusion | flops 404422656 | bytes 3216384 | tf_op jit(solution)/shard_map/dot_general | solution.py:69
  16.3 0.0 reduce-scatter.4.cloned.1.call-update
  16.3 0.0 all-gather.3.cloned.1.call-start
  16.4 0.6 copy-done.7
  16.9 0.1 copy.34
  17.1 0.2 reshape.98
  17.3 2.4 reduce-window.6
  19.7 0.1 slice.43
  19.9 0.1 copy.36
  20.0 0.1 reshape.135
  20.2 0.1 bitcast_bitcast_fusion
  20.3 0.1 fusion.26
  20.4 1.2 scatter_custom_fusion
  21.6 26.1 %reduce-scatter.4.cloned.1.call-done = bf16[96,2048]{1,0:T(8,128)(2,1)} async-done(((bf16[384,2048]{1,0:T(8,128)(2,1)}), bf16[96,2048]{1,0:T(8,128)(2,1)}) %reduce-scatter.4.cloned.1.call-update) | async-done | bytes 393232 | tf_op jit(solution)/shard_map/reduce_scatter | solution.py:68
  47.8 1.2 fusion.7
  49.0 1.2 fusion.9
  50.2 0.7 copy-done.3
  51.0 1.4 gather_fusion
  52.3 0.4 reshape.102
  52.8 39.5 %all_to_all.15 = bf16[64,4,2048]{2,1,0:T(4,128)(2,1)S(1)} all-to-all(bf16[64,4,2048]{2,1,0:T(4,128)(2,1)S(1)} %reshape.102), channel_id=1, replica_groups=mesh['sp'=64,'tp'=4] {'sp'}, dimensions={0} | all-to-all | bytes 2097152 | tf_op jit(solution)/shard_map/all_to_all | solution.py:90
  92.3 1.6 copy.39
  93.8 0.0 reduce-scatter.8.cloned.1.call-start
  93.9 46.1 %all-gather.3.cloned.1.call-done = bf16[64,16,2048]{2,0,1:T(8,128)(2,1)} async-done(((bf16[64,4,2048]{2,0,1:T(8,128)(2,1)}), bf16[64,16,2048]{2,0,1:T(8,128)(2,1)}) %all-gather.3.cloned.1.call-update) | async-done | bytes 4194320 | tf_op jit(solution)/shard_map/all_gather | solution.py:93
  140.0 3.6 %convolution_bitcast_fusion.1 = f32[64,1,16,256]{3,0,2,1:T(8,128)S(1)} fusion(bf16[64,16,2048]{2,0,1:T(8,128)(2,1)} %all-gather.3.cloned.1.call-done, bf16[1,2048,256]{2,1,0:T(8,128)(2,1)S(1)} %copy-done.9), kind=kOutput, calls=%fused_computation.9 | convolution fusion | flops 1073741824 | bytes 6291456 | tf_op jit(solution)/shard_map/gerd,edf->gerf/dot_general | solution.py:96
  143.6 1.3 fusion.2
  144.9 1.4 convert_bitcast_fusion
  146.3 4.2 %copy.41 = bf16[64,1,16,2048]{3,0,1,2:T(8,128)(2,1)} copy(bf16[64,1,16,2048]{3,2,0,1:T(8,128)(2,1)S(1)} %convert_bitcast_fusion) | data formatting | bytes 8388608 | tf_op jit(solution)/shard_map/optimization_barrier | solution.py:19
  150.5 0.0 reduce-scatter.8.cloned.1.call-update
  150.5 0.0 reduce-scatter.6.cloned.1.call-start
  150.6 0.9 copy-done.4
  151.5 0.2 stack.2
  151.7 31.0 %all_to_all.16 = bf16[4,96,2048]{2,1,0:T(8,128)(2,1)S(1)} all-to-all(bf16[4,96,2048]{2,1,0:T(8,128)(2,1)S(1)} %stack.2), channel_id=1, replica_groups=mesh['sp'=64,'tp'=4] {'tp'}, dimensions={0} | all-to-all | bytes 3145728 | tf_op jit(solution)/shard_map/all_to_all | solution.py:9
  182.7 0.6 fusion.38
  183.3 4.5 %convolution_convert_fusion = bf16[384,2048]{1,0:T(8,128)(2,1)} fusion(bf16[256,2048]{1,0:T(8,128)(2,1)} %param.29, bf16[384,2048]{1,0:T(8,128)(2,1)S(1)} %bitcast.69, bf16[2048,256]{1,0:T(8,128)(2,1)} %param.28, f32[384,256]{1,0:T(8,128)S(1)} %fusion.38), kind=kOutput, calls=%fused_computation.4 | convolution fusion | flops 806682624 | bytes 5636096 | tf_op jit(solution)/shard_map/dot_general | solution.py:108
  187.8 23.0 %reduce-scatter.8.cloned.1.call-done = bf16[64,1,4,2048]{3,0,1,2:T(8,128)(2,1)} async-done(((bf16[64,1,16,2048]{3,0,1,2:T(8,128)(2,1)}), bf16[64,1,4,2048]{3,0,1,2:T(8,128)(2,1)}) %reduce-scatter.8.cloned.1.call-update) | async-done | bytes 1048592 | tf_op jit(solution)/shard_map/reduce_scatter | solution.py:111
  210.8 3.0 %copy.42 = bf16[64,1,4,2048]{3,2,1,0:T(4,128)(2,1)} copy(bf16[64,1,4,2048]{3,0,1,2:T(8,128)(2,1)} %reduce-scatter.8.cloned.1.call-done) | data formatting | bytes 2097152 | tf_op jit(solution)/shard_map/reduce_scatter | solution.py:111
  213.8 10.4 %all-to-all-start.2 = ((bf16[64,1,4,2048]{3,2,1,0:T(4,128)(2,1)}), bf16[64,1,4,2048]{3,2,1,0:T(4,128)(2,1)S(1)}, u32[]{:S(2)}, u32[]{:S(2)}) async-start(bf16[64,1,4,2048]{3,2,1,0:T(4,128)(2,1)} %copy.42), calls=%async_computation.5 | async-start | bytes 2097152 | tf_op jit(solution)/shard_map/all_to_all | solution.py:118
  224.3 0.8 constant_dynamic-slice_fusion
  225.0 0.7 copy.43
  225.7 26.7 %all-to-all-done.2 = bf16[64,1,4,2048]{3,2,1,0:T(4,128)(2,1)S(1)} async-done(((bf16[64,1,4,2048]{3,2,1,0:T(4,128)(2,1)}), bf16[64,1,4,2048]{3,2,1,0:T(4,128)(2,1)S(1)}, u32[]{:S(2)}, u32[]{:S(2)}) %all-to-all-start.2) | async-done | bytes 1048608 | tf_op jit(solution)/shard_map/all_to_all | solution.py:118
  252.4 0.3 reshape.109
  252.7 2.0 gather_fusion.1
  254.7 2.2 reshape.114
  256.9 3.2 %multiply_reduce_fusion = f32[96,2048]{1,0:T(8,128)} fusion(f32[96,2,2048]{2,1,0:T(2,128)S(1)} %reshape.114, f32[96,2]{1,0:T(8,128)S(1)} %copy-done.5), kind=kLoop, calls=%fused_computation.6 | loop fusion | flops 589824 | bytes 2360064 | tf_op jit(solution)/shard_map/reduce_sum | solution.py:124
  260.1 2.2 fusion.11
  (39 shorter events, 0.2 us)
Async XLA Ops:
  6.5 138.4 %copy-start = (bf16[1,256,2048]{2,1,0:T(8,128)(2,1)S(1)}, bf16[1,256,2048]{2,1,0:T(8,128)(2,1)}, u32[]{:S(2)}) copy-start(bf16[1,256,2048]{2,1,0:T(8,128)(2,1)} %param.26) | copy-start | bytes 3145732
  6.5 41.2 %reduce-scatter.4.cloned.1.call-start = ((), (), s32[]{:S(2)}) async-start(), calls=%async_computation.6 | async-start | bytes 1966080 | tf_op jit(solution)/shard_map/reduce_scatter | solution.py:68
  7.7 5.4 %collective-permute-start = (f32[2,256]{1,0:T(2,128)S(1)}, f32[2,256]{1,0:T(2,128)S(1)}, u32[]{:S(2)}, u32[]{:S(2)}) collective-permute-start(f32[2,256]{1,0:T(2,128)S(1)} %slice.40), channel_id=1, source_target_pairs={{0,4},{4,8},{8,12},{12,16},{16,20},{20,24},{24,28},{28,32},{32,36}... | collective-permute-start | bytes 6152 | tf_op jit(solution)/shard_map/ppermute | solution.py:15
  16.3 0.7 copy-start.7
  16.3 31.5 %copy-start.1 = (bf16[96,2048]{1,0:T(8,128)(2,1)S(1)}, bf16[96,2048]{1,0:T(8,128)(2,1)}, u32[]{:S(2)}) copy-start(bf16[96,2048]{1,0:T(8,128)(2,1)} %param.15) | copy-start | bytes 1179652
  16.3 123.7 %all-gather.3.cloned.1.call-start = ((), (), s32[]{:S(2)}) async-start(), calls=%async_computation.9 | async-start | bytes 5242880 | tf_op jit(solution)/shard_map/all_gather | solution.py:93
  17.3 31.7 %copy-start.6 = (f32[2048]{0:T(1024)S(1)}, f32[2048]{0:T(1024)}, u32[]{:S(2)}) copy-start(f32[2048]{0:T(1024)} %param.21) | copy-start | bytes 24580
  50.2 0.7 copy-start.3
  92.3 47.7 %copy-start.9 = (bf16[1,2048,256]{2,1,0:T(8,128)(2,1)S(1)}, bf16[1,2048,256]{2,1,0:T(8,128)(2,1)}, u32[]{:S(2)}) copy-start(bf16[1,2048,256]{2,1,0:T(8,128)(2,1)} %param.24) | copy-start | bytes 3145732
  93.8 49.7 %copy-start.10 = (bf16[1,2048,256]{2,1,0:T(8,128)(2,1)S(1)}, bf16[1,2048,256]{2,1,0:T(8,128)(2,1)}, u32[]{:S(2)}) copy-start(bf16[1,2048,256]{2,1,0:T(8,128)(2,1)} %param.25) | copy-start | bytes 3145732
  93.8 117.0 %reduce-scatter.8.cloned.1.call-start = ((), (), s32[]{:S(2)}) async-start(), calls=%async_computation.8 | async-start | bytes 5242880 | tf_op jit(solution)/shard_map/reduce_scatter | solution.py:111
  140.0 3.6 %copy-start.8 = (bf16[64,16,2048]{2,0,1:T(8,128)(2,1)S(1)}, bf16[64,16,2048]{2,0,1:T(8,128)(2,1)}, u32[]{:S(2)}) copy-start(bf16[64,16,2048]{2,0,1:T(8,128)(2,1)} %all-gather.3.cloned.1.call-done) | copy-start | bytes 12582916
  150.5 1.0 copy-start.4
  150.5 109.6 %reduce-scatter.6.cloned.1.call-start = ((), (), s32[]{:S(2)}) async-start(), calls=%async_computation.7 | async-start | bytes 1966080 | tf_op jit(solution)/shard_map/reduce_scatter | solution.py:114
  151.7 31.0 %copy-start.11 = (bf16[2048,256]{1,0:T(8,128)(2,1)S(1)}, bf16[2048,256]{1,0:T(8,128)(2,1)}, u32[]{:S(2)}) copy-start(bf16[2048,256]{1,0:T(8,128)(2,1)} %param.27) | copy-start | bytes 3145732
  213.8 38.6 %all-to-all-start.2 = ((bf16[64,1,4,2048]{3,2,1,0:T(4,128)(2,1)}), bf16[64,1,4,2048]{3,2,1,0:T(4,128)(2,1)S(1)}, u32[]{:S(2)}, u32[]{:S(2)}) async-start(bf16[64,1,4,2048]{3,2,1,0:T(4,128)(2,1)} %copy.42), calls=%async_computation.5 | async-start | bytes 2097152 | tf_op jit(solution)/shard_map/all_to_all | solution.py:118
  254.7 2.2 copy-start.5
  256.9 3.2 %copy-start.2 = (bf16[96,2048]{1,0:T(8,128)(2,1)S(1)}, bf16[96,2048]{1,0:T(8,128)(2,1)}, u32[]{:S(2)}) copy-start(bf16[96,2048]{1,0:T(8,128)(2,1)} %reduce-scatter.4.cloned.1.call-done) | copy-start | bytes 1179652
Sparse Core Ops, SparseCore 0:
  16.4 31.3 reduce-scatter.3
  94.0 45.9 all-gather.2
  150.7 60.0 reduce-scatter.7
  213.2 26.8 reduce-scatter.5
